TPU v7x, 32 devices: a whole 2x2x4 slice. The times are simulated.
32 devices in a mesh: sp: 8 (over z, x), tp: 4 (over y, core).
Axes of the slice: x: 2, y: 2, z: 4, core: 2. Of those that a mesh axis runs over, the one named last changes fastest.
Arguments:
- resid: bfloat16 [1024, 2048], P('sp'), may hold values from -8 to 8
- a_val: bfloat16 [1024, 1024], P('sp', 'tp'), may hold values from -8 to 8
- a_gate: bfloat16 [1024, 1024], P('sp', 'tp'), may hold values from -6 to 6
- conv_kernel: bfloat16 [31, 1024], P(None, 'tp'), may hold values from -1 to 1
- conv_bias: float32 [1024], P('tp'), may hold values from -3 to 3
- ln_gain: float32 [1024], P('tp'), may hold values from 0.1 to 1.9
- ln_bias: float32 [1024], P('tp'), may hold values from -3 to 3
- w_out: bfloat16 [1024, 2048], P('tp'), may hold values from -0.1875 to 0.1875
- ffn_gain: float32 [2048], replicated, may hold values from 0.1 to 1.9
- routes: int32 [1024, 4], P('sp'), may hold values from 0 to 7, all different within a row; in each aligned block of 128 rows (0 to 127, 128 to 255, ...) at most 128 rows name the same one
- route_weights: float32 [1024, 4], P('sp'), may hold values from 0.15 to 1.2
- exp_gate: bfloat16 [8, 2048, 4096], P('sp', None, 'tp'), may hold values from -0.125 to 0.125
- exp_up: bfloat16 [8, 2048, 4096], P('sp', None, 'tp'), may hold values from -0.125 to 0.125
- exp_down: bfloat16 [8, 4096, 2048], P('sp', None, 'tp'), may hold values from -0.09375 to 0.09375
- sh_gate: bfloat16 [2048, 512], P(None, 'tp'), may hold values from -0.125 to 0.125
- sh_up: bfloat16 [2048, 512], P(None, 'tp'), may hold values from -0.125 to 0.125
- sh_down: bfloat16 [512, 2048], P(None, 'tp'), may hold values from -0.25 to 0.25
Outputs:
- result: bfloat16 [1024, 2048], P('sp', 'tp')
Inputs may be any that keep to these rules, and one draw needn't show every extreme that they name: `routes`: among the 128 rows of one index of sp, each expert is named at most 128 times, a bound that some block reaches; a row names 4 different experts.
All inputs are finite; a program needn't handle non-finite values.
Results may differ from a plain program's by a relative error of at most 0.007.
Values may be sent and summed in bfloat16 or wider, within the bound.
A program may use at most 64 MiB of HBM per device.

v0:
```python
import jax
import jax.numpy as jnp
from jax import lax
from jax.sharding import PartitionSpec as P

LN_EPS = 1e-05
RMS_EPS = 1e-06


def shifted(value, axis, by):
    size = lax.axis_size(axis)
    pairs = [(i, i + by) for i in range(size) if 0 <= i + by < size]
    return lax.ppermute(value, axis, pairs)


def body(
    resid,
    a_val,
    a_gate,
    conv_kernel,
    conv_bias,
    ln_gain,
    ln_bias,
    w_out,
    ffn_gain,
    routes,
    route_weights,
    exp_gate,
    exp_up,
    exp_down,
    sh_gate,
    sh_up,
    sh_down,
):
    tp_count = lax.axis_size("tp")
    tp_place = lax.axis_index("tp")
    sp_count = lax.axis_size("sp")
    tok_rows = resid.shape[0]
    model_width = resid.shape[1]
    col_width = model_width // tp_count
    col_start = tp_place * col_width
    conv_span = conv_kernel.shape[0]
    channels_all = a_val.shape[1] * tp_count
    gated_in = (a_val.astype(jnp.float32) * jax.nn.sigmoid(a_gate.astype(jnp.float32))).astype(
        jnp.bfloat16
    )
    before = shifted(gated_in[tok_rows - (conv_span - 1) :], "sp", 1)
    padded = jnp.concatenate([before, gated_in], axis=0).astype(jnp.float32)
    kernel = conv_kernel.astype(jnp.float32)

    def add_tap(offset, running):
        window_rows = lax.dynamic_slice_in_dim(padded, offset, tok_rows, 0)
        return running + lax.dynamic_slice_in_dim(kernel, offset, 1, 0) * window_rows

    start_sum = jnp.broadcast_to(conv_bias[None, :], gated_in.shape)
    conv_out = lax.fori_loop(0, conv_span, add_tap, start_sum)
    row_sums = lax.psum((jnp.sum(conv_out, axis=1), jnp.sum(conv_out * conv_out, axis=1)), "tp")
    channel_mean = row_sums[0] / channels_all
    channel_var = row_sums[1] / channels_all - channel_mean * channel_mean
    scaled = (conv_out - channel_mean[:, None]) * lax.rsqrt(
        channel_var[:, None] + LN_EPS
    ) * ln_gain[None, :] + ln_bias[None, :]
    mixed_out = jax.nn.silu(scaled).astype(jnp.bfloat16)
    partial_proj = jnp.dot(mixed_out, w_out, preferred_element_type=jnp.float32)
    projected = lax.psum(partial_proj, "tp")
    middle = (resid.astype(jnp.float32) + projected).astype(jnp.bfloat16)
    middle_f = middle.astype(jnp.float32)
    inverse = lax.rsqrt(jnp.mean(middle_f * middle_f, axis=1, keepdims=True) + RMS_EPS)
    normed = (middle_f * inverse * ffn_gain[None, :]).astype(jnp.bfloat16)
    middle_cols = lax.dynamic_slice_in_dim(middle, col_start, col_width, 1)
    shared_gate = jnp.dot(normed, sh_gate, preferred_element_type=jnp.float32)
    shared_up = jnp.dot(normed, sh_up, preferred_element_type=jnp.float32)
    shared_hidden = (jax.nn.silu(shared_gate) * shared_up).astype(jnp.bfloat16)
    weight_rows = sh_down
    shared = jnp.dot(
        lax.all_gather(shared_hidden, "tp", axis=1, tiled=True),
        weight_rows,
        preferred_element_type=jnp.float32,
    )
    top_count = routes.shape[1]
    local_experts = exp_gate.shape[0]
    experts_all = local_experts * sp_count
    capacity = max(2 * tok_rows * top_count // experts_all, tp_count)
    pair_count = tok_rows * top_count
    chosen = routes.reshape(pair_count)
    one_hot = (chosen[:, None] == jnp.arange(experts_all, dtype=jnp.int32)[None, :]).astype(
        jnp.int32
    )
    earlier = jnp.cumsum(one_hot, axis=0) - one_hot
    place_in = jnp.sum(earlier * one_hot, axis=1)
    slot_of = chosen * capacity + place_in
    owner_ids = (
        jnp.zeros((experts_all * capacity,), jnp.int32)
        .at[slot_of]
        .set(jnp.arange(pair_count, dtype=jnp.int32) + 1)
    )
    owner_grid = owner_ids.reshape(sp_count, local_experts, capacity)
    part_slots = capacity // tp_count
    own_owners = lax.dynamic_slice_in_dim(owner_grid, tp_place * part_slots, part_slots, 2)
    source_row = jnp.maximum(own_owners - 1, 0) // top_count
    taken = normed[source_row.reshape(-1)].reshape(own_owners.shape + (model_width,))
    landed = lax.all_to_all(
        jnp.where((own_owners > 0)[..., None], taken, jnp.zeros((), jnp.bfloat16)),
        "sp",
        split_axis=0,
        concat_axis=0,
        tiled=True,
    )
    arrived = lax.all_gather(landed, "tp", axis=2, tiled=True)
    gate_part = jnp.einsum("sxcd,xdf->sxcf", arrived, exp_gate, preferred_element_type=jnp.float32)
    up_part = jnp.einsum("sxcd,xdf->sxcf", arrived, exp_up, preferred_element_type=jnp.float32)
    expert_hidden = (jax.nn.silu(gate_part) * up_part).astype(jnp.bfloat16)
    weight_rows = exp_down
    expert_sum = jnp.einsum(
        "sxcf,xfd->sxcd",
        lax.all_gather(expert_hidden, "tp", axis=3, tiled=True),
        weight_rows,
        preferred_element_type=jnp.float32,
    )
    expert_out = expert_sum.astype(jnp.bfloat16)
    returned = lax.all_to_all(expert_out, "sp", split_axis=0, concat_axis=0, tiled=True)
    flat_out = returned.reshape(experts_all * capacity, col_width)
    picked = flat_out[slot_of].astype(jnp.float32).reshape(tok_rows, top_count, col_width)
    routed = jnp.sum(picked * route_weights[:, :, None], axis=1)
    return (middle_cols.astype(jnp.float32) + shared + routed).astype(jnp.bfloat16)


def solution(mesh):
    in_specs = (
        P("sp", None),
        P("sp", "tp"),
        P("sp", "tp"),
        P(None, "tp"),
        P("tp"),
        P("tp"),
        P("tp"),
        P("tp", None),
        P(),
        P("sp", None),
        P("sp", None),
        P("sp", None, "tp"),
        P("sp", None, "tp"),
        P("sp", None, "tp"),
        P(None, "tp"),
        P(None, "tp"),
        P(None, "tp"),
    )
    out_specs = P("sp", "tp")
    return jax.shard_map(body, mesh=mesh, in_specs=in_specs, out_specs=out_specs, check_vma=False)
```

profile of v0, /device:TPU:0, one launch (start us, length us, event | category | flops | bytes accessed | tf_op | source)
XLA Modules:
  0.0 262.0 jit_solution(12313480295030517520)
XLA Ops:
  6.5 0.0 copy-start
  6.5 0.0 copy-start.1
  6.5 0.0 all-reduce.3.cloned.1.call-start
  6.5 1.0 multiply_convert_fusion.1
  7.6 4.9 %collective-permute-start = (bf16[30,256]{1,0:T(8,128)(2,1)S(1)}, bf16[30,256]{1,0:T(8,128)(2,1)S(1)}, u32[]{:S(2)}, u32[]{:S(2)}) collective-permute-start(bf16[30,256]{1,0:T(8,128)(2,1)S(1)} %slice.16), channel_id=1, source_target_pairs={{0,4},{4,8},{8,12},{12,16},{16,20},{20,24},{24,28},{1,5},{5,9},{9,... | collective-permute-start | bytes 46088 | tf_op jit(solution)/shard_map/ppermute | solution.py:13
  12.5 0.7 broadcast_multiply_fusion
  13.2 0.8 copy.24
  13.9 0.1 eq.29
  14.1 0.1 eq.25
  14.2 0.0 copy-start.2
  14.2 0.1 copy.23
  14.3 0.1 mul.137
  14.4 1.1 reduce-window.6
  15.6 0.2 slice_reduce_fusion
  15.8 0.1 fusion.40
  15.9 0.7 convert_element_type.69
  16.7 2.4 scatter_custom_fusion
  19.1 0.0 collective-permute-done
  19.1 0.7 broadcast_in_dim.14
  19.8 2.4 while.13
  22.3 0.1 fusion.46
  22.4 6.3 %all-reduce = (f32[128]{0:T(128)S(1)}, f32[128]{0:T(128)S(1)}) all-reduce(f32[128]{0:T(128)S(1)} %get-tuple-element.86, f32[128]{0:T(128)S(1)} %get-tuple-element.85), channel_id=1, replica_groups=mesh['sp'=8,'tp'=4] {'tp'}, use_global_device_ids=true, to_apply=%region_5.0 | all-reduce | flops 256 | bytes 2048 | tf_op jit(solution)/shard_map/psum | solution.py:57
  28.7 0.0 copy-done
  28.7 2.1 fusion.33
  30.8 0.0 all-reduce.3.cloned.1.call-update
  30.9 0.0 all-gather.3.cloned.1.call-start
  30.9 0.1 add_select_fusion
  31.0 0.1 reshape.144
  31.1 0.1 compare_bitcast_fusion
  31.2 36.0 %all-reduce.3.cloned.1.call-done = f32[128,2048]{1,0:T(8,128)} async-done(((f32[128,2048]{1,0:T(8,128)}), f32[128,2048]{1,0:T(8,128)}) %all-reduce.3.cloned.1.call-update) | async-done | bytes 1048592 | tf_op jit(solution)/shard_map/psum | solution.py:65
  67.2 0.0 copy-done.1
  67.2 1.5 fusion.30
  68.7 0.0 copy-done.2
  68.7 0.2 fusion.32
  68.9 1.4 gather_fusion
  70.2 0.1 broadcast_select_fusion
  70.4 30.6 %all_to_all.10 = bf16[8,1,32,2048]{3,2,1,0:T(8,128)(2,1)} all-to-all(bf16[8,1,32,2048]{3,2,1,0:T(8,128)(2,1)S(1)} %broadcast_select_fusion), channel_id=1, replica_groups=mesh['sp'=8,'tp'=4] {'sp'}, dimensions={0} | all-to-all | bytes 2097152 | tf_op jit(solution)/shard_map/all_to_all | solution.py:102
  101.0 0.0 all-gather.3.cloned.1.call-update
  101.1 0.0 all-gather.5.cloned.1.call-start
  101.1 33.4 %all-gather.3.cloned.1.call-done = bf16[8,1,128,2048]{3,2,0,1:T(8,128)(2,1)} async-done(((bf16[8,1,32,2048]{3,2,0,1:T(8,128)(2,1)}), bf16[8,1,128,2048]{3,2,0,1:T(8,128)(2,1)}) %all-gather.3.cloned.1.call-update) | async-done | bytes 4194320 | tf_op jit(solution)/shard_map/all_gather | solution.py:109
  134.5 0.0 copy-start.4
  134.5 0.0 copy-start.5
  134.6 7.7 %fusion.4 = f32[8,128,1024]{2,1,0:T(8,128)S(1)} fusion(bf16[1,2048,1024]{2,1,0:T(8,128)(2,1)} %param.31, bf16[8,1,128,2048]{3,2,0,1:T(8,128)(2,1)} %all-gather.3.cloned.1.call-done), kind=kOutput, calls=%fused_computation.10 | convolution fusion | flops 4294967296 | bytes 12582912 | tf_op jit(solution)/shard_map/sxcd,xdf->sxcf/dot_general | solution.py:111
  142.2 0.0 copy-done.4
  142.2 0.0 copy-done.5
  142.2 6.4 %fusion.2 = bf16[8,1,128,1024]{3,2,0,1:T(8,128)(2,1)} fusion(f32[8,128,1024]{2,1,0:T(8,128)S(1)} %fusion.4, bf16[1,2048,1024]{2,1,0:T(8,128)(2,1)S(1)} %copy-done.4, bf16[8,1,128,2048]{3,2,0,1:T(8,128)(2,1)S(1)} %copy-done.5), kind=kOutput, calls=%fused_computation.8 | convolution fusion | flops 4301258752 | bytes 14680064 | tf_op jit(solution)/shard_map/sxcd,xdf->sxcf/dot_general | solution.py:110
  148.6 0.0 all-gather.5.cloned.1.call-update
  148.6 0.0 copy-start.3
  148.6 58.4 %all-gather.5.cloned.1.call-done = bf16[8,1,128,4096]{3,2,0,1:T(8,128)(2,1)} async-done(((bf16[8,1,128,1024]{3,2,0,1:T(8,128)(2,1)}), bf16[8,1,128,4096]{3,2,0,1:T(8,128)(2,1)}) %all-gather.5.cloned.1.call-update) | async-done | bytes 8388624 | tf_op jit(solution)/shard_map/all_gather | solution.py:116
  207.0 10.1 %fusion.22 = bf16[8,1,128,512]{3,2,1,0:T(8,128)(2,1)} fusion(bf16[1,4096,512]{2,1,0:T(8,128)(2,1)} %param.32, bf16[8,1,128,4096]{3,2,0,1:T(8,128)(2,1)} %all-gather.5.cloned.1.call-done), kind=kOutput, calls=%fused_computation.22 | convolution fusion | flops 4295491584 | bytes 13631488 | tf_op jit(solution)/shard_map/sxcf,xfd->sxcd/dot_general | solution.py:114
  217.2 5.5 %all-to-all-start.1 = ((bf16[8,1,128,512]{3,2,1,0:T(8,128)(2,1)}), bf16[8,1,128,512]{3,2,1,0:T(8,128)(2,1)S(1)}, u32[]{:S(2)}, u32[]{:S(2)}) async-start(bf16[8,1,128,512]{3,2,1,0:T(8,128)(2,1)} %fusion.22), calls=%async_computation.1 | async-start | bytes 2097152 | tf_op jit(solution)/shard_map/all_to_all | solution.py:121
  222.7 0.0 copy-done.3
  222.7 0.1 copy.29
  222.8 1.3 fusion.47
  224.1 1.3 fusion.29
  225.5 5.4 %all_gather.9 = bf16[128,512]{1,0:T(8,128)(2,1)S(1)} all-gather(bf16[128,128]{1,0:T(8,128)(2,1)S(1)} %fusion.29), channel_id=1, replica_groups=mesh['sp'=8,'tp'=4] {'tp'}, dimensions={1}, use_global_device_ids=true | all-gather | bytes 163840 | tf_op jit(solution)/shard_map/all_gather | solution.py:76
  230.9 17.9 %all-to-all-done.1 = bf16[8,1,128,512]{3,2,1,0:T(8,128)(2,1)S(1)} async-done(((bf16[8,1,128,512]{3,2,1,0:T(8,128)(2,1)}), bf16[8,1,128,512]{3,2,1,0:T(8,128)(2,1)S(1)}, u32[]{:S(2)}, u32[]{:S(2)}) %all-to-all-start.1) | async-done | bytes 1048608 | tf_op jit(solution)/shard_map/all_to_all | solution.py:121
  248.9 2.6 gather_fusion.1
  251.5 1.4 reshape.152
  252.8 0.7 multiply_reduce_fusion
  253.6 1.9 fusion.28
  (74 shorter events, 1.6 us)
Async XLA Ops:
  6.5 22.2 %copy-start = (bf16[256,2048]{1,0:T(8,128)(2,1)S(1)}, bf16[256,2048]{1,0:T(8,128)(2,1)}, u32[]{:S(2)}) copy-start(bf16[256,2048]{1,0:T(8,128)(2,1)} %param.26) | copy-start | bytes 3145732
  6.5 60.7 %copy-start.1 = (bf16[128,2048]{1,0:T(8,128)(2,1)S(1)}, bf16[128,2048]{1,0:T(8,128)(2,1)}, u32[]{:S(2)}) copy-start(bf16[128,2048]{1,0:T(8,128)(2,1)} %param.19) | copy-start | bytes 1572868
  6.5 60.6 %all-reduce.3.cloned.1.call-start = ((), (), s32[]{:S(2)}) async-start(), calls=%async_computation.2 | async-start | bytes 2097152 | tf_op jit(solution)/shard_map/psum | solution.py:65
  7.6 11.5 %collective-permute-start = (bf16[30,256]{1,0:T(8,128)(2,1)S(1)}, bf16[30,256]{1,0:T(8,128)(2,1)S(1)}, u32[]{:S(2)}, u32[]{:S(2)}) collective-permute-start(bf16[30,256]{1,0:T(8,128)(2,1)S(1)} %slice.16), channel_id=1, source_target_pairs={{0,4},{4,8},{8,12},{12,16},{16,20},{20,24},{24,28},{1,5},{5,9},{9,... | collective-permute-start | bytes 46088 | tf_op jit(solution)/shard_map/ppermute | solution.py:13
  14.2 54.5 %copy-start.2 = (f32[2048]{0:T(1024)S(1)}, f32[2048]{0:T(1024)}, u32[]{:S(2)}) copy-start(f32[2048]{0:T(1024)} %param.27) | copy-start | bytes 24580
  30.9 103.7 %all-gather.3.cloned.1.call-start = ((), (), s32[]{:S(2)}) async-start(), calls=%async_computation.3 | async-start | bytes 5242880 | tf_op jit(solution)/shard_map/all_gather | solution.py:109
  101.1 106.0 %all-gather.5.cloned.1.call-start = ((), (), s32[]{:S(2)}) async-start(), calls=%async_computation.4 | async-start | bytes 10485760 | tf_op jit(solution)/shard_map/all_gather | solution.py:116
  134.5 7.7 %copy-start.4 = (bf16[1,2048,1024]{2,1,0:T(8,128)(2,1)S(1)}, bf16[1,2048,1024]{2,1,0:T(8,128)(2,1)}, u32[]{:S(2)}) copy-start(bf16[1,2048,1024]{2,1,0:T(8,128)(2,1)} %param.30) | copy-start | bytes 12582916
  134.5 7.7 %copy-start.5 = (bf16[8,1,128,2048]{3,2,0,1:T(8,128)(2,1)S(1)}, bf16[8,1,128,2048]{3,2,0,1:T(8,128)(2,1)}, u32[]{:S(2)}) copy-start(bf16[8,1,128,2048]{3,2,0,1:T(8,128)(2,1)} %all-gather.3.cloned.1.call-done) | copy-start | bytes 12582916
  148.6 74.0 %copy-start.3 = (f32[128,4]{0,1:T(4,128)S(1)}, f32[128,4]{0,1:T(4,128)}, u32[]{:S(2)}) copy-start(f32[128,4]{0,1:T(4,128)} %param.29) | copy-start | bytes 6148
  217.2 31.7 %all-to-all-start.1 = ((bf16[8,1,128,512]{3,2,1,0:T(8,128)(2,1)}), bf16[8,1,128,512]{3,2,1,0:T(8,128)(2,1)S(1)}, u32[]{:S(2)}, u32[]{:S(2)}) async-start(bf16[8,1,128,512]{3,2,1,0:T(8,128)(2,1)} %fusion.22), calls=%async_computation.1 | async-start | bytes 2097152 | tf_op jit(solution)/shard_map/all_to_all | solution.py:121
Sparse Core Ops, SparseCore 0:
  31.0 36.1 all-reduce.2
  101.2 33.3 all-gather.2
  148.7 58.2 all-gather.4
where the time goes:
time: 263 us; the launch traced here: 262 us
  waiting for transfers between devices  146 us (56%)
  blocking collectives  42.4 us (16%)
  matrix products  30.9 us (12%)
  between operations  13.3 us (5%)
  starting transfers between devices  10.5 us (4%)
  local copies, waits for them, and re-layouts  10.4 us (4%)
  other arithmetic  7.78 us (3%)
    all_gather x1, waiting for transfers between devices, body(): lax.all_gather(expert_hidden, 'tp', axis=3, tiled=True)  58.4 us
    psum x1, waiting for transfers between devices, body(): projected = lax.psum(partial_proj, 'tp')  36 us
    all_gather x1, waiting for transfers between devices, body(): arrived = lax.all_gather(landed, 'tp', axis=2, tiled=True)  33.4 us
    all_to_all x1, blocking collectives, body(): lax.all_to_all(jnp.where((own_owners > 0)[..., None], taken, jnp.zeros(()...  30.6 us
    all_to_all x1, waiting for transfers between devices, body(): lax.all_to_all(expert_out, 'sp', split_axis=0, concat_axis=0, tiled=True)  17.9 us
    dot_general x1, matrix products, body(): jnp.einsum('sxcf,xfd->sxcd', lax.all_gather(expert_hidden, 'tp', axis=3,...  10.1 us
    dot_general x1, matrix products, body(): jnp.einsum('sxcd,xdf->sxcf', arrived, exp_up, preferred_element_type=jnp....  7.65 us
    dot_general x1, matrix products, body(): jnp.einsum('sxcd,xdf->sxcf', arrived, exp_gate, preferred_element_type=jn...  6.37 us
  transfers between devices with their start and end apart: 5, of which 4 were waited for; matrix products, arithmetic and copies ran while one was open for 4% of the time, Pallas kernels for 0%

commit v1 on v0

--- a/solution.py
+++ b/solution.py
@@ -2,6 +2,7 @@
 import jax.numpy as jnp
 from jax import lax
 from jax.sharding import PartitionSpec as P
+from jax.lax import all_gather
 
 LN_EPS = 1e-05
 RMS_EPS = 1e-06
@@ -111,9 +112,14 @@
     up_part = jnp.einsum("sxcd,xdf->sxcf", arrived, exp_up, preferred_element_type=jnp.float32)
     expert_hidden = (jax.nn.silu(gate_part) * up_part).astype(jnp.bfloat16)
     weight_rows = exp_down
+
+    def wall_group(content, axis_key):
+        r_now = all_gather(content, axis_key)
+        return jnp.concatenate(r_now, 3)
+
     expert_sum = jnp.einsum(
         "sxcf,xfd->sxcd",
-        lax.all_gather(expert_hidden, "tp", axis=3, tiled=True),
+        wall_group(expert_hidden, "tp"),
         weight_rows,
         preferred_element_type=jnp.float32,
     )

time: 263 us -> 290 us (1.10)
  local copies, waits for them, and re-layouts: 10.4 us -> 36.9 us
    another operation x1 -> x2, local copies, waits for them, and re-layouts: 0.01 us -> 14.4 us
    all_gather x0 -> x1, local copies, waits for them, and re-layouts: none -> 12.2 us  [wall_group(): r_now = all_gather(content, axis_key)]
  transfers between devices with their start and end apart: 5 -> 5, of which waited for: 4 -> 4; matrix products, arithmetic and copies ran while one was open for 4% -> 3% of each run, Pallas kernels for 0% -> 0%
where the time goes in v1:
time: 290 us; the launch traced here: 289 us
  waiting for transfers between devices  146 us (50%)
  blocking collectives  42.4 us (15%)
  local copies, waits for them, and re-layouts  36.9 us (13%)
  matrix products  30.9 us (11%)
  between operations  13.3 us (5%)
  starting transfers between devices  10.6 us (4%)
  other arithmetic  7.79 us (3%)
    all_gather x1, waiting for transfers between devices, wall_group(): r_now = all_gather(content, axis_key)  58.4 us
    psum x1, waiting for transfers between devices, body(): projected = lax.psum(partial_proj, 'tp')  36 us
    all_gather x1, waiting for transfers between devices, body(): arrived = lax.all_gather(landed, 'tp', axis=2, tiled=True)  33.3 us
    all_to_all x1, blocking collectives, body(): lax.all_to_all(jnp.where((own_owners > 0)[..., None], taken, jnp.zeros(()...  30.6 us
    all_to_all x1, waiting for transfers between devices, body(): lax.all_to_all(expert_out, 'sp', split_axis=0, concat_axis=0, tiled=True)  18 us
    another operation x2, local copies, waits for them, and re-layouts  14.4 us
    all_gather x1, local copies, waits for them, and re-layouts, wall_group(): r_now = all_gather(content, axis_key)  12.2 us
    dot_general x1, matrix products, body(): jnp.einsum('sxcf,xfd->sxcd', wall_group(expert_hidden, 'tp'), weight_rows...  10.1 us
  transfers between devices with their start and end apart: 5, of which 4 were waited for; matrix products, arithmetic and copies ran while one was open for 3% of the time, Pallas kernels for 0%

profile of v1, /device:TPU:0, one launch (start us, length us, event | category | flops | bytes accessed | tf_op | source)
XLA Modules:
  0.0 288.6 jit_solution(15837828662458275867)
XLA Ops:
  6.5 0.0 copy-start
  6.5 0.0 copy-start.1
  6.5 0.0 all-reduce.3.cloned.1.call-start
  6.5 1.0 multiply_convert_fusion.1
  7.6 4.9 %collective-permute-start = (bf16[30,256]{1,0:T(8,128)(2,1)S(1)}, bf16[30,256]{1,0:T(8,128)(2,1)S(1)}, u32[]{:S(2)}, u32[]{:S(2)}) collective-permute-start(bf16[30,256]{1,0:T(8,128)(2,1)S(1)} %slice.16), channel_id=1, source_target_pairs={{0,4},{4,8},{8,12},{12,16},{16,20},{20,24},{24,28},{1,5},{5,9},{9,... | collective-permute-start | bytes 46088 | tf_op jit(solution)/shard_map/ppermute | solution.py:14
  12.5 0.7 broadcast_multiply_fusion
  13.2 0.8 copy.26
  13.9 0.1 eq.29
  14.1 0.1 eq.25
  14.2 0.0 copy-start.2
  14.2 0.1 copy.25
  14.3 0.1 mul.137
  14.4 1.1 reduce-window.6
  15.6 0.2 slice_reduce_fusion
  15.8 0.1 fusion.40
  15.9 0.7 convert_element_type.69
  16.7 2.4 scatter_custom_fusion
  19.1 0.0 collective-permute-done
  19.1 0.7 broadcast_in_dim.14
  19.8 2.4 while.13
  22.3 0.1 fusion.46
  22.4 6.3 %all-reduce = (f32[128]{0:T(128)S(1)}, f32[128]{0:T(128)S(1)}) all-reduce(f32[128]{0:T(128)S(1)} %get-tuple-element.86, f32[128]{0:T(128)S(1)} %get-tuple-element.85), channel_id=1, replica_groups=mesh['sp'=8,'tp'=4] {'tp'}, use_global_device_ids=true, to_apply=%region_5.0 | all-reduce | flops 256 | bytes 2048 | tf_op jit(solution)/shard_map/psum | solution.py:58
  28.7 0.0 copy-done
  28.7 2.1 fusion.33
  30.8 0.0 all-reduce.3.cloned.1.call-update
  30.9 0.0 all-gather.4.cloned.1.call-start
  30.9 0.1 add_select_fusion
  31.0 0.1 reshape.149
  31.1 0.1 compare_bitcast_fusion
  31.2 36.0 %all-reduce.3.cloned.1.call-done = f32[128,2048]{1,0:T(8,128)} async-done(((f32[128,2048]{1,0:T(8,128)}), f32[128,2048]{1,0:T(8,128)}) %all-reduce.3.cloned.1.call-update) | async-done | bytes 1048592 | tf_op jit(solution)/shard_map/psum | solution.py:66
  67.2 0.0 copy-done.1
  67.2 1.5 fusion.30
  68.7 0.0 copy-done.2
  68.7 0.2 fusion.32
  68.9 1.4 gather_fusion
  70.2 0.1 broadcast_select_fusion
  70.4 30.6 %all_to_all.10 = bf16[8,1,32,2048]{3,2,1,0:T(8,128)(2,1)} all-to-all(bf16[8,1,32,2048]{3,2,1,0:T(8,128)(2,1)S(1)} %broadcast_select_fusion), channel_id=1, replica_groups=mesh['sp'=8,'tp'=4] {'sp'}, dimensions={0} | all-to-all | bytes 2097152 | tf_op jit(solution)/shard_map/all_to_all | solution.py:103
  101.0 0.0 all-gather.4.cloned.1.call-update
  101.0 0.2 all-gather.6.cloned.1.call-start
  101.3 33.3 %all-gather.4.cloned.1.call-done = bf16[8,1,128,2048]{3,2,0,1:T(8,128)(2,1)} async-done(((bf16[8,1,32,2048]{3,2,0,1:T(8,128)(2,1)}), bf16[8,1,128,2048]{3,2,0,1:T(8,128)(2,1)}) %all-gather.4.cloned.1.call-update) | async-done | bytes 4194320 | tf_op jit(solution)/shard_map/all_gather | solution.py:110
  134.5 0.0 copy-start.4
  134.5 0.0 copy-start.5
  134.5 7.6 %fusion.3 = f32[8,128,1024]{2,1,0:T(8,128)S(1)} fusion(bf16[1,2048,1024]{2,1,0:T(8,128)(2,1)} %param.31, bf16[8,1,128,2048]{3,2,0,1:T(8,128)(2,1)} %all-gather.4.cloned.1.call-done), kind=kOutput, calls=%fused_computation.10 | convolution fusion | flops 4294967296 | bytes 12582912 | tf_op jit(solution)/shard_map/sxcd,xdf->sxcf/dot_general | solution.py:112
  142.2 0.0 copy-done.4
  142.2 0.0 copy-done.5
  142.2 6.4 %fusion.16 = bf16[8,1,128,1024]{3,2,1,0:T(8,128)(2,1)} fusion(f32[8,128,1024]{2,1,0:T(8,128)S(1)} %fusion.3, bf16[1,2048,1024]{2,1,0:T(8,128)(2,1)S(1)} %copy-done.4, bf16[8,1,128,2048]{3,2,0,1:T(8,128)(2,1)S(1)} %copy-done.5), kind=kOutput, calls=%fused_computation.21 | convolution fusion | flops 4301258752 | bytes 14680064 | tf_op jit(solution)/shard_map/sxcd,xdf->sxcf/dot_general | solution.py:111
  148.6 0.0 all-gather.6.cloned.1.call-update
  148.6 58.4 %all-gather.6.cloned.1.call-done = bf16[32,1,128,1024]{3,2,1,0:T(8,128)(2,1)} async-done(((bf16[8,1,128,1024]{3,2,1,0:T(8,128)(2,1)}), bf16[32,1,128,1024]{3,2,1,0:T(8,128)(2,1)}) %all-gather.6.cloned.1.call-update) | async-done | bytes 8388624 | tf_op jit(solution)/shard_map/all_gather | solution.py:117
  207.0 12.2 %copy.35 = bf16[4,8,1,128,1024]{4,0,3,1,2:T(4,128)(2,1)} copy(bf16[4,8,1,128,1024]{4,3,1,0,2:T(8,128)(2,1)} %bitcast.109) | data formatting | bytes 16777216 | tf_op jit(solution)/shard_map/all_gather | solution.py:117
  219.2 14.4 %reshape.155 = bf16[8,128,4096]{2,1,0:T(8,128)(2,1)} reshape(bf16[8,1,128,4,1024]{4,3,2,0,1:T(4,128)(2,1)} %bitcast.107) | data formatting | bytes 16777216 | tf_op jit(solution)/shard_map/reshape.19
  233.5 0.0 copy-start.3
  233.5 10.1 %fusion.24 = bf16[8,1,128,512]{3,2,1,0:T(8,128)(2,1)} fusion(bf16[8,128,4096]{2,1,0:T(8,128)(2,1)} %reshape.155, bf16[1,4096,512]{2,1,0:T(8,128)(2,1)} %param.32), kind=kOutput, calls=%fused_computation.23 | convolution fusion | flops 4295491584 | bytes 13631488 | tf_op jit(solution)/shard_map/sxcf,xfd->sxcd/dot_general | solution.py:120
  243.7 5.5 %all-to-all-start.1 = ((bf16[8,1,128,512]{3,2,1,0:T(8,128)(2,1)}), bf16[8,1,128,512]{3,2,1,0:T(8,128)(2,1)S(1)}, u32[]{:S(2)}, u32[]{:S(2)}) async-start(bf16[8,1,128,512]{3,2,1,0:T(8,128)(2,1)} %fusion.24), calls=%async_computation.1 | async-start | bytes 2097152 | tf_op jit(solution)/shard_map/all_to_all | solution.py:127
  249.2 0.0 copy-done.3
  249.2 0.1 copy.33
  249.3 1.3 fusion.47
  250.6 1.3 fusion.29
  252.0 5.4 %all_gather.12 = bf16[128,512]{1,0:T(8,128)(2,1)S(1)} all-gather(bf16[128,128]{1,0:T(8,128)(2,1)S(1)} %fusion.29), channel_id=1, replica_groups=mesh['sp'=8,'tp'=4] {'tp'}, dimensions={1}, use_global_device_ids=true | all-gather | bytes 163840 | tf_op jit(solution)/shard_map/all_gather | solution.py:77
  257.4 18.0 %all-to-all-done.1 = bf16[8,1,128,512]{3,2,1,0:T(8,128)(2,1)S(1)} async-done(((bf16[8,1,128,512]{3,2,1,0:T(8,128)(2,1)}), bf16[8,1,128,512]{3,2,1,0:T(8,128)(2,1)S(1)}, u32[]{:S(2)}, u32[]{:S(2)}) %all-to-all-start.1) | async-done | bytes 1048608 | tf_op jit(solution)/shard_map/all_to_all | solution.py:127
  275.4 2.6 gather_fusion.1
  278.0 1.4 reshape.158
  279.4 0.7 multiply_reduce_fusion
  280.1 1.9 fusion.28
  (74 shorter events, 1.6 us)
Async XLA Ops:
  6.5 22.2 %copy-start = (bf16[256,2048]{1,0:T(8,128)(2,1)S(1)}, bf16[256,2048]{1,0:T(8,128)(2,1)}, u32[]{:S(2)}) copy-start(bf16[256,2048]{1,0:T(8,128)(2,1)} %param.26) | copy-start | bytes 3145732
  6.5 60.6 %copy-start.1 = (bf16[128,2048]{1,0:T(8,128)(2,1)S(1)}, bf16[128,2048]{1,0:T(8,128)(2,1)}, u32[]{:S(2)}) copy-start(bf16[128,2048]{1,0:T(8,128)(2,1)} %param.19) | copy-start | bytes 1572868
  6.5 60.6 %all-reduce.3.cloned.1.call-start = ((), (), s32[]{:S(2)}) async-start(), calls=%async_computation.2 | async-start | bytes 2097152 | tf_op jit(solution)/shard_map/psum | solution.py:66
  7.6 11.5 %collective-permute-start = (bf16[30,256]{1,0:T(8,128)(2,1)S(1)}, bf16[30,256]{1,0:T(8,128)(2,1)S(1)}, u32[]{:S(2)}, u32[]{:S(2)}) collective-permute-start(bf16[30,256]{1,0:T(8,128)(2,1)S(1)} %slice.16), channel_id=1, source_target_pairs={{0,4},{4,8},{8,12},{12,16},{16,20},{20,24},{24,28},{1,5},{5,9},{9,... | collective-permute-start | bytes 46088 | tf_op jit(solution)/shard_map/ppermute | solution.py:14
  14.2 54.5 %copy-start.2 = (f32[2048]{0:T(1024)S(1)}, f32[2048]{0:T(1024)}, u32[]{:S(2)}) copy-start(f32[2048]{0:T(1024)} %param.27) | copy-start | bytes 24580
  30.9 103.7 %all-gather.4.cloned.1.call-start = ((), (), s32[]{:S(2)}) async-start(), calls=%async_computation.3 | async-start | bytes 5242880 | tf_op jit(solution)/shard_map/all_gather | solution.py:110
  101.0 106.0 %all-gather.6.cloned.1.call-start = ((), (), s32[]{:S(2)}) async-start(), calls=%async_computation.4 | async-start | bytes 10485760 | tf_op jit(solution)/shard_map/all_gather | solution.py:117
  134.5 7.7 %copy-start.4 = (bf16[1,2048,1024]{2,1,0:T(8,128)(2,1)S(1)}, bf16[1,2048,1024]{2,1,0:T(8,128)(2,1)}, u32[]{:S(2)}) copy-start(bf16[1,2048,1024]{2,1,0:T(8,128)(2,1)} %param.30) | copy-start | bytes 12582916
  134.5 7.7 %copy-start.5 = (bf16[8,1,128,2048]{3,2,0,1:T(8,128)(2,1)S(1)}, bf16[8,1,128,2048]{3,2,0,1:T(8,128)(2,1)}, u32[]{:S(2)}) copy-start(bf16[8,1,128,2048]{3,2,0,1:T(8,128)(2,1)} %all-gather.4.cloned.1.call-done) | copy-start | bytes 12582916
  233.5 15.7 %copy-start.3 = (f32[128,4]{0,1:T(4,128)S(1)}, f32[128,4]{0,1:T(4,128)}, u32[]{:S(2)}) copy-start(f32[128,4]{0,1:T(4,128)} %param.29) | copy-start | bytes 6148
  243.7 31.7 %all-to-all-start.1 = ((bf16[8,1,128,512]{3,2,1,0:T(8,128)(2,1)}), bf16[8,1,128,512]{3,2,1,0:T(8,128)(2,1)S(1)}, u32[]{:S(2)}, u32[]{:S(2)}) async-start(bf16[8,1,128,512]{3,2,1,0:T(8,128)(2,1)} %fusion.24), calls=%async_computation.1 | async-start | bytes 2097152 | tf_op jit(solution)/shard_map/all_to_all | solution.py:127
Sparse Core Ops, SparseCore 0:
  31.0 36.1 all-reduce.2
  101.2 33.3 all-gather.3
  148.7 58.2 all-gather.5
